TPU v7x, 32 devices: a whole 2x2x4 slice. The times are simulated.
32 devices in a mesh: ep: 8 (over z, x), tp: 4 (over y, core).
Axes of the slice: x: 2, y: 2, z: 4, core: 2. Of those that a mesh axis runs over, the one named last changes fastest.
Arguments:
- tokens: bfloat16 [64, 2048], P('ep', 'tp'), may hold values from -10 to 10, as said below
- norm_gain: float32 [2048], P('tp'), may hold values from 0.5 to 1.5
- norm_bias: float32 [2048], P('tp'), may hold values from -0.3 to 0.3
- group_pick: int32 [64, 1], P('ep'), may hold values from 0 to 1; in each aligned block of 8 rows (0 to 7, 8 to 15, ...) at most 4 rows name the same one
- member_pick: int32 [64, 4], P('ep'), may hold values from 0 to 7, all different within a row
- picked_probs: float32 [64, 4], P('ep'), may hold values from 0.05 to 1
- gate_weight: bfloat16 [16, 2048, 1024], P('ep', 'tp'), may hold values from -0.125 to 0.125
- up_weight: bfloat16 [16, 2048, 1024], P('ep', 'tp'), may hold values from -0.125 to 0.125
- down_weight: bfloat16 [16, 1024, 2048], P('ep', None, 'tp'), may hold values from -0.375 to 0.375
Outputs:
- mixed: bfloat16 [64, 2048], P('ep', 'tp')
Inputs may be any that keep to these rules, and one draw needn't show every extreme that they name: `group_pick`: each entry is a group number from 0 to 1; within each aligned block of 8 tokens no group is named by more than 4 tokens, a bound that some block reaches. `member_pick`: each token's 4 entries are different member numbers from 0 to 7. `tokens`: each token is its own offset between -2 and 2 plus its own scale between 0.25 and 2 times entries of at most 4 in size.
All inputs are finite; a program needn't handle non-finite values.
Results may differ from a plain program's by a relative error of at most 0.01.
Values may be sent and summed in bfloat16 or wider, within the bound.
A program may use at most 64 MiB of HBM per device.

v0:
```python
import jax
import jax.numpy as jnp
from jax import lax
from jax.sharding import PartitionSpec as P

EPG = 8


norm_epsilon = 1e-05


def normalize(tokens, norm_gain, norm_bias):
    values = tokens.astype(jnp.float32)
    features = values.shape[1] * lax.axis_size("tp")
    first_sums, square_sums = lax.psum(
        (jnp.sum(values, axis=1, keepdims=True), jnp.sum(values * values, axis=1, keepdims=True)),
        "tp",
    )
    center = first_sums / features
    shifted = values - center
    spread = square_sums / features - center * center
    scaled = shifted * lax.rsqrt(spread + norm_epsilon)
    return (scaled * norm_gain.astype(jnp.float32) + norm_bias.astype(jnp.float32)).astype(
        jnp.bfloat16
    )


def membership(labels, number):
    levels = lax.broadcasted_iota(jnp.int32, (1, 1, number), 2)
    return jnp.any(labels[:, :, None] == levels, axis=1).astype(jnp.int32)


def earlier_counts(present):
    return (jnp.cumsum(present, axis=0) - present).astype(jnp.int32)


def placement(present, slots, capacity):
    levels = lax.broadcasted_iota(jnp.int32, (1, 1, capacity), 2)
    hits = present[:, :, None] * (slots[:, :, None] == levels).astype(jnp.int32)
    return hits.reshape(present.shape[0], -1).astype(jnp.bfloat16)


def pack_rows(placed, normed):
    return jnp.einsum("tp,td->pd", placed, normed, preferred_element_type=jnp.float32).astype(
        jnp.bfloat16
    )


def activate(gate_full, up_full):
    return (jax.nn.silu(gate_full) * up_full).astype(jnp.bfloat16)


def project_down(hidden, down_weight):
    return jnp.einsum(
        "jrf,jfd->jrd", hidden, down_weight, preferred_element_type=jnp.float32
    ).astype(jnp.bfloat16)


def by_source(results, peers, capacity):
    local_experts = results.shape[0]
    width = results.shape[2]
    parted = results.reshape(local_experts, peers, capacity, width)
    return jnp.transpose(parted, (1, 0, 2, 3)).reshape(peers, local_experts * capacity, width)


def combine(returned, positions, shares):
    picked = jnp.take(returned, positions, axis=0)
    return jnp.sum(shares[:, :, None] * picked.astype(jnp.float32), axis=1).astype(jnp.bfloat16)


def per_device(
    tokens,
    norm_gain,
    norm_bias,
    group_pick,
    member_pick,
    picked_probs,
    gate_weight,
    up_weight,
    down_weight,
):
    normed = normalize(tokens, norm_gain, norm_bias)
    token_count = tokens.shape[0]
    shard_width = tokens.shape[1]
    local_experts = gate_weight.shape[0]
    peers = lax.axis_size("ep")
    experts = local_experts * peers
    groups = experts // EPG
    capacity = max(token_count // 4, (token_count + groups - 1) // groups)
    chosen = (group_pick * EPG + member_pick).astype(jnp.int32)
    shares = picked_probs / jnp.sum(picked_probs, axis=1, keepdims=True)
    present = membership(chosen, experts)
    slots = earlier_counts(present)
    outgoing = pack_rows(placement(present, slots, capacity), normed)
    outgoing = outgoing.reshape(peers, local_experts * capacity, shard_width)
    incoming = lax.all_to_all(outgoing, "ep", split_axis=0, concat_axis=0, tiled=True)
    rows = incoming.reshape(peers, local_experts, capacity, shard_width)
    rows = jnp.transpose(rows, (1, 0, 2, 3)).reshape(local_experts, peers * capacity, shard_width)
    gate_part = jnp.einsum("jrd,jdf->jrf", rows, gate_weight, preferred_element_type=jnp.float32)
    up_part = jnp.einsum("jrd,jdf->jrf", rows, up_weight, preferred_element_type=jnp.float32)
    gate_full, up_full = lax.psum((gate_part, up_part), "tp")
    results = project_down(activate(gate_full, up_full), down_weight)
    returned = lax.all_to_all(
        by_source(results, peers, capacity), "ep", split_axis=0, concat_axis=0, tiled=True
    )
    positions = chosen * capacity + jnp.take_along_axis(slots, chosen, axis=1)
    mixed = combine(returned.reshape(experts * capacity, shard_width), positions, shares)
    return mixed


def solution(mesh):
    placed = (
        P("ep", "tp"),
        P("tp"),
        P("tp"),
        P("ep", None),
        P("ep", None),
        P("ep", None),
        P("ep", "tp", None),
        P("ep", "tp", None),
        P("ep", None, "tp"),
    )
    return jax.shard_map(
        per_device, mesh=mesh, in_specs=placed, out_specs=P("ep", "tp"), check_vma=False
    )
```

profile of v0, /device:TPU:0, one launch (start us, length us, event | category | flops | bytes accessed | tf_op | source)
XLA Modules:
  0.0 89.0 jit_solution(11475215240998323717)
XLA Ops:
  6.5 0.8 multiply_bitcast_fusion
  7.3 0.8 convert_reduce_fusion
  8.2 0.8 copy.34
  9.0 0.1 clamp_shift-left_fusion
  9.0 0.1 copy.35
  9.1 0.1 fusion.9
  9.2 0.1 copy.39
  9.3 0.1 copy.38
  9.4 0.1 eq.39
  9.5 8.4 %all-reduce = (f32[8,1]{0,1:T(1,128)S(1)}, f32[8,1]{0,1:T(1,128)S(1)}) all-reduce(f32[8,1]{0,1:T(1,128)S(1)} %bitcast.34, f32[8,1]{0,1:T(1,128)S(1)} %bitcast.33), channel_id=1, replica_groups=mesh['ep'=8,'tp'=4] {'tp'}, use_global_device_ids=true, to_apply=%region_6.0 | all-reduce | flops 16 | bytes 128 | tf_op jit(solution)/shard_map/psum | solution.py:15
  17.9 1.6 %fusion = bf16[8,8,512]{2,1,0:T(8,128)(2,1)} fusion(s32[8,64]{0,1:T(8,128)S(1)} %bitcast.31, s32[8,64]{0,1:T(8,128)S(1)} %bitcast.32, s32[64]{0:T(128)S(1)} %eq.39, bf16[8,512]{1,0:T(8,128)(2,1)} %param.9, f32[512]{0:T(512)} %param.11, f32[512]{0:T(512)} %param.10, f32[8]{0:T(128)S(1)} %get-tuple-element.16, f32[8]{0:T(128)S(1)} %get-tuple-element.15), kind=kOutput, calls=%fused_computation.4 | convolution fusion | flops 583168 | bytes 82240 | tf_op jit(solution)/shard_map/tp,td->pd/dot_general | solution.py:44
  19.5 5.8 %all-to-all-start = ((bf16[8,8,512]{2,1,0:T(8,128)(2,1)}), bf16[8,8,512]{2,1,0:T(8,128)(2,1)S(1)}, u32[]{:S(2)}, u32[]{:S(2)}) async-start(bf16[8,8,512]{2,1,0:T(8,128)(2,1)} %fusion), calls=%async_computation | async-start | bytes 131072 | tf_op jit(solution)/shard_map/all_to_all | solution.py:96
  25.3 0.0 all-reduce.4.cloned.1.call-start
  25.3 0.1 copy.36
  25.4 6.8 %all-to-all-done = bf16[8,8,512]{2,1,0:T(8,128)(2,1)S(1)} async-done(((bf16[8,8,512]{2,1,0:T(8,128)(2,1)}), bf16[8,8,512]{2,1,0:T(8,128)(2,1)S(1)}, u32[]{:S(2)}, u32[]{:S(2)}) %all-to-all-start) | async-done | bytes 65568 | tf_op jit(solution)/shard_map/all_to_all | solution.py:96
  32.3 1.2 %fusion.18 = f32[2,32,1024]{2,1,0:T(8,128)} fusion(bf16[2,32,512]{2,1,0:T(8,128)(2,1)S(1)} %reshape.52, bf16[2,512,1024]{2,1,0:T(8,128)(2,1)S(1)} %copy-done), kind=kOutput, calls=%fused_computation.41 | convolution fusion | flops 67108864 | bytes 2424832 | tf_op jit(solution)/shard_map/jrd,jdf->jrf/dot_general | solution.py:100
  33.5 0.5 copy-done.1
  34.0 1.2 %fusion.17 = f32[2,32,1024]{2,1,0:T(8,128)} fusion(bf16[2,32,512]{2,1,0:T(8,128)(2,1)S(1)} %reshape.52, bf16[2,512,1024]{2,1,0:T(8,128)(2,1)S(1)} %copy-done.1), kind=kOutput, calls=%fused_computation.40 | convolution fusion | flops 67108864 | bytes 2424832 | tf_op jit(solution)/shard_map/jrd,jdf->jrf/dot_general | solution.py:99
  35.2 0.0 all-reduce.4.cloned.1.call-update
  35.2 0.1 copy.37
  35.3 0.1 reshape.64
  35.4 0.7 gather_fusion.1
  36.1 0.1 reshape.67
  36.2 29.3 %all-reduce.4.cloned.1.call-done = (f32[2,32,1024]{2,1,0:T(8,128)}, f32[2,32,1024]{2,1,0:T(8,128)}) async-done(((f32[2,32,1024]{2,1,0:T(8,128)}, f32[2,32,1024]{2,1,0:T(8,128)}), (f32[2,32,1024]{2,1,0:T(8,128)}, f32[2,32,1024]{2,1,0:T(8,128)})) %all-reduce.4.cloned.1.call-update) | async-done | bytes 524304 | tf_op jit(solution)/shard_map/psum | solution.py:101
  65.5 2.2 %convolution_convert_fusion.1 = bf16[2,32,512]{2,1,0:T(8,128)(2,1)S(1)} fusion(bf16[2,1024,512]{2,1,0:T(8,128)(2,1)} %param.17, f32[2,32,1024]{2,1,0:T(8,128)} %get-tuple-element.9, f32[2,32,1024]{2,1,0:T(8,128)} %get-tuple-element.10), kind=kOutput, calls=%fused_computation.3 | convolution fusion | flops 67534848 | bytes 2686976 | tf_op jit(solution)/shard_map/jrf,jfd->jrd/dot_general | solution.py:54
  67.7 0.6 copy.42
  68.4 5.5 %all-to-all-start.1 = ((bf16[8,8,512]{2,1,0:T(8,128)(2,1)}), bf16[8,8,512]{2,1,0:T(8,128)(2,1)S(1)}, u32[]{:S(2)}, u32[]{:S(2)}) async-start(bf16[8,8,512]{2,1,0:T(8,128)(2,1)} %copy.42), calls=%async_computation.1 | async-start | bytes 131072 | tf_op jit(solution)/shard_map/all_to_all | solution.py:103
  73.9 0.1 copy.33
  74.0 0.1 reshape.58
  74.1 6.7 %all-to-all-done.1 = bf16[8,8,512]{2,1,0:T(8,128)(2,1)S(1)} async-done(((bf16[8,8,512]{2,1,0:T(8,128)(2,1)}), bf16[8,8,512]{2,1,0:T(8,128)(2,1)S(1)}, u32[]{:S(2)}, u32[]{:S(2)}) %all-to-all-start.1) | async-done | bytes 65568 | tf_op jit(solution)/shard_map/all_to_all | solution.py:103
  80.8 0.6 gather_fusion
  81.4 0.7 multiply_reduce_fusion
  (23 shorter events, 0.3 us)
Async XLA Ops:
  6.5 25.8 %copy-start = (bf16[2,512,1024]{2,1,0:T(8,128)(2,1)S(1)}, bf16[2,512,1024]{2,1,0:T(8,128)(2,1)}, u32[]{:S(2)}) copy-start(bf16[2,512,1024]{2,1,0:T(8,128)(2,1)} %param.16) | copy-start | bytes 6291460
  19.5 12.7 %all-to-all-start = ((bf16[8,8,512]{2,1,0:T(8,128)(2,1)}), bf16[8,8,512]{2,1,0:T(8,128)(2,1)S(1)}, u32[]{:S(2)}, u32[]{:S(2)}) async-start(bf16[8,8,512]{2,1,0:T(8,128)(2,1)} %fusion), calls=%async_computation | async-start | bytes 131072 | tf_op jit(solution)/shard_map/all_to_all | solution.py:96
  25.3 40.2 %all-reduce.4.cloned.1.call-start = ((), (), s32[]{:S(2)}) async-start(), calls=%async_computation.2 | async-start | bytes 1048576 | tf_op jit(solution)/shard_map/psum | solution.py:101
  32.3 1.7 %copy-start.1 = (bf16[2,512,1024]{2,1,0:T(8,128)(2,1)S(1)}, bf16[2,512,1024]{2,1,0:T(8,128)(2,1)}, u32[]{:S(2)}) copy-start(bf16[2,512,1024]{2,1,0:T(8,128)(2,1)} %param.15) | copy-start | bytes 6291460
  35.4 0.8 copy-start.2
  68.4 12.4 %all-to-all-start.1 = ((bf16[8,8,512]{2,1,0:T(8,128)(2,1)}), bf16[8,8,512]{2,1,0:T(8,128)(2,1)S(1)}, u32[]{:S(2)}, u32[]{:S(2)}) async-start(bf16[8,8,512]{2,1,0:T(8,128)(2,1)} %copy.42), calls=%async_computation.1 | async-start | bytes 131072 | tf_op jit(solution)/shard_map/all_to_all | solution.py:103
Sparse Core Ops, SparseCore 0:
  35.3 30.1 all-reduce.3
where the time goes:
time: 89.5 us; the launch traced here: 89 us
  waiting for transfers between devices  42.8 us (48%)
  between operations  13.5 us (15%)
  starting transfers between devices  11.4 us (13%)
  blocking collectives  8.44 us (9%)
  matrix products  6.1 us (7%)
  local copies, waits for them, and re-layouts  4.16 us (5%)
  other arithmetic  2.63 us (3%)
    psum x1, waiting for transfers between devices, per_device(): gate_full, up_full = lax.psum((gate_part, up_part), 'tp')  29.3 us
    psum x1, blocking collectives, normalize(): lax.psum((jnp.sum(values, axis=1, keepdims=True), jnp.sum(values * values...  8.44 us
    all_to_all x1, waiting for transfers between devices, per_device(): lax.all_to_all(outgoing, 'ep', split_axis=0, concat_axis=0, tiled=True)  6.78 us
    all_to_all x1, waiting for transfers between devices, per_device(): lax.all_to_all(by_source(results, peers, capacity), 'ep', split_axis=0, c...  6.73 us
    all_to_all x1, starting transfers between devices, per_device(): lax.all_to_all(outgoing, 'ep', split_axis=0, concat_axis=0, tiled=True)  5.81 us
    all_to_all x1, starting transfers between devices, per_device(): lax.all_to_all(by_source(results, peers, capacity), 'ep', split_axis=0, c...  5.51 us
    dot_general x1, matrix products, project_down(): jnp.einsum('jrf,jfd->jrd', hidden, down_weight, preferred_element_type=jn...  2.18 us
  transfers between devices with their start and end apart: 3, of which 3 were waited for; matrix products, arithmetic and copies ran while one was open for 1% of the time, Pallas kernels for 0%

commit v1 on v0

v1 whole, which is shorter than its diff:
```python
import functools

import jax
import jax.numpy as jnp
from jax import lax
from jax.experimental import pallas as pl
from jax.experimental.pallas import tpu as pltpu
from jax.sharding import PartitionSpec as P

EPG = 8
CORES = 2
LANES = 128
norm_epsilon = 1e-05
MESH = pl.DeviceIdType.MESH
F32 = jnp.float32
BF16 = jnp.bfloat16


def iota(shape, dim):
    return lax.broadcasted_iota(jnp.int32, shape, dim)


def kernel(
    E, T, G, cap,
    tokens_h, gain_h, bias_h, group_h, member_h, probs_h, gate_h, up_h, down_h,
    out_ref,
    tokens_v, gain_v, bias_v, group_v, member_v, probs_v, gate_v, up_v, down_v,
    stat_buf, share_out, share_in, share_all, rows_out, rows_in, rows_all,
    core_out, core_in, y_out, y_in, held, hid_own, hid_other, back_out, back_in,
    local_sem, weight_sem,
    stat_s, stat_r, share_s, share_r, rows_s, rows_r,
    core_s, core_r, y_s, y_r, hid_s, hid_r, back_s, back_r,
):
    n, width = tokens_h.shape
    LE = gate_h.shape[0]
    FF = gate_h.shape[2]
    half = FF // CORES
    NY = T // CORES
    S = G * cap
    R = E * cap
    group_devices = EPG // LE
    me = lax.axis_index("ep")
    mt = lax.axis_index("tp")
    core = lax.rem(mt, CORES)
    my = lax.div(mt, CORES)

    def ep_at(d):
        return lax.rem(me + d, E)

    def tp_at(d):
        return lax.rem(mt + d, T)

    def remote(src, dst, ssem, rsem, ep, tp):
        return pltpu.make_async_remote_copy(
            src_ref=src, dst_ref=dst, send_sem=ssem, recv_sem=rsem,
            device_id=(ep, tp), device_id_type=MESH,
        )

    barrier = pltpu.get_barrier_semaphore()
    for d in range(1, E):
        pl.semaphore_signal(barrier, inc=1, device_id=(ep_at(d), mt), device_id_type=MESH)
    for d in range(1, T):
        pl.semaphore_signal(barrier, inc=1, device_id=(me, tp_at(d)), device_id_type=MESH)

    small = [
        pltpu.make_async_copy(h, v, local_sem.at[i])
        for i, (h, v) in enumerate(
            ((group_h, group_v), (member_h, member_v), (probs_h, probs_v),
             (tokens_h, tokens_v), (gain_h, gain_v), (bias_h, bias_v))
        )
    ]
    for c in small:
        c.start()
    weights = [
        [pltpu.make_async_copy(h.at[j], v.at[j], weight_sem.at[w, j]) for j in range(LE)]
        for w, (h, v) in enumerate(((gate_h, gate_v), (up_h, up_v), (down_h, down_v)))
    ]
    for w in range(2):
        for j in range(LE):
            weights[w][j].start()
    for j in range(LE):
        weights[2][j].start()
    for c in small:
        c.wait()

    lane = iota((n, LANES), 1)
    sub = iota((n, LANES), 0)
    group = group_v[...].astype(F32)
    group_wide = jnp.broadcast_to(group, (n, LANES))
    group_row = jnp.sum(jnp.where(lane == sub, group_wide, 0.0), axis=0, keepdims=True)
    same = jnp.where(group_wide == group_row, 1.0, 0.0)
    slot_row = jnp.sum(jnp.where(sub < lane, same, 0.0), axis=0, keepdims=True)
    slot_col = jnp.sum(jnp.where(lane < sub, same, 0.0), axis=1, keepdims=True)
    key_row = jnp.where(iota((1, LANES), 1) < n, group_row * cap + slot_row, -1.0)
    key_col = group * cap + slot_col
    place = jnp.where(key_row == iota((S, LANES), 0).astype(F32), 1.0, 0.0)

    def pack(v):
        total = place[:, 0:1] * v[0:1, :]
        for t in range(1, n):
            total += place[:, t : t + 1] * v[t : t + 1, :]
        return total

    probs = probs_v[...]
    member = member_v[...]
    shares = probs / jnp.sum(probs, axis=1, keepdims=True)
    share_tile = jnp.zeros((n, LANES), F32)
    for k in range(probs.shape[1]):
        share_tile += jnp.where(lane == member[:, k : k + 1], shares[:, k : k + 1], 0.0)
    share_tile = pack(share_tile)
    for g in range(G):
        share_out[g] = share_tile[g * cap : (g + 1) * cap, :]

    values = pack(tokens_v[...].astype(F32))
    center_here = jnp.sum(values, axis=1, keepdims=True) / width
    away = values - center_here
    square_here = jnp.sum(away * away, axis=1, keepdims=True)
    slane = iota((S, LANES), 1)
    stat_buf[0] = jnp.where(slane == 0, center_here, jnp.where(slane == 1, square_here, 0.0))

    pl.semaphore_wait(barrier, E + T - 2)

    stat = [
        remote(stat_buf.at[0], stat_buf.at[d], stat_s.at[d - 1], stat_r.at[d - 1], me, tp_at(d))
        for d in range(1, T)
    ]
    for c in stat:
        c.start()
    share = []
    for d in range(1, E):
        p = ep_at(d)
        c = remote(
            share_out.at[lax.div(p, group_devices)], share_in.at[d],
            share_s.at[d - 1], share_r.at[d - 1], p, mt,
        )
        c.start()
        share.append(c)
    share_in[0] = share_out[lax.div(me, group_devices)]
    gain = gain_v[...]
    bias = bias_v[...]
    for c in stat:
        c.wait_recv()
    stats = [stat_buf[d] for d in range(T)]
    center = sum(s[:, 0:1] for s in stats) / T
    square = sum(s[:, 1:2] + width * (s[:, 0:1] - center) * (s[:, 0:1] - center) for s in stats)
    spread = square / (width * T)
    normed = (values - center) * lax.rsqrt(spread + norm_epsilon) * gain + bias
    for g in range(G):
        rows_out[g] = normed[g * cap : (g + 1) * cap, :].astype(BF16)

    sent = []
    for d in range(1, E):
        p = ep_at(d)
        c = remote(
            rows_out.at[lax.div(p, group_devices)], rows_in.at[d],
            rows_s.at[d - 1], rows_r.at[d - 1], p, mt,
        )
        c.start()
        sent.append(c)
    rows_in[0] = rows_out[lax.div(me, group_devices)]
    rows_all[0:cap, :] = rows_in[0].astype(F32)
    for w in range(2):
        for j in range(LE):
            weights[w][j].wait()
    for d in range(1, E):
        sent[d - 1].wait_recv()
        rows_all[d * cap : (d + 1) * cap, :] = rows_in[d].astype(F32)
    rows = rows_all[...].astype(BF16)

    mine = pl.ds(pl.multiple_of(core * half, half), half)
    theirs = pl.ds(pl.multiple_of((1 - core) * half, half), half)
    partner = my * CORES + (1 - core)
    to_core = []
    for j in range(LE):
        for w, v in enumerate((gate_v, up_v)):
            core_out[j, w] = jnp.dot(rows, v[j, :, theirs], preferred_element_type=F32).astype(BF16)
        c = remote(core_out.at[j], core_in.at[j], core_s.at[j], core_r.at[j], me, partner)
        c.start()
        to_core.append(c)
    to_y = []
    for j in range(LE):
        for w, v in enumerate((gate_v, up_v)):
            held[j, w] = jnp.dot(rows, v[j, :, mine], preferred_element_type=F32)
        to_core[j].wait_recv()
        for w in range(2):
            total = held[j, w] + core_in[j, w].astype(F32)
            held[j, w] = total
            y_out[j, w] = total.astype(BF16)
        copies = []
        for d in range(1, NY):
            c = remote(
                y_out.at[j], y_in.at[j, d - 1], y_s.at[j, d - 1], y_r.at[j, d - 1],
                me, lax.rem(my + d, NY) * CORES + core,
            )
            c.start()
            copies.append(c)
        to_y.append(copies)
    for d in range(1, E):
        share[d - 1].wait_recv()
    for d in range(E):
        share_all[d * cap : (d + 1) * cap, :] = share_in[d]
    for j in range(LE):
        weights[2][j].wait()
    to_hid = []
    partial = []
    for j in range(LE):
        gate = held[j, 0]
        up = held[j, 1]
        for d in range(1, NY):
            to_y[j][d - 1].wait_recv()
            gate += y_in[j, d - 1, 0].astype(F32)
            up += y_in[j, d - 1, 1].astype(F32)
        hidden = (gate / (1.0 + jnp.exp(-gate)) * up).astype(BF16)
        hid_own[j] = hidden
        c = remote(hid_own.at[j], hid_other.at[j], hid_s.at[j], hid_r.at[j], me, partner)
        c.start()
        to_hid.append(c)
        partial.append(jnp.dot(hidden, down_v[j, mine, :], preferred_element_type=F32))
    total = jnp.zeros((R, width), F32)
    rlane = iota((R, LANES), 1)
    weight_tile = share_all[...]
    for j in range(LE):
        to_hid[j].wait_recv()
        expert = partial[j] + jnp.dot(hid_other[j], down_v[j, theirs, :], preferred_element_type=F32)
        which = lax.rem(me * LE + j, EPG)
        weight = jnp.sum(jnp.where(rlane == which, weight_tile, 0.0), axis=1, keepdims=True)
        total += weight * expert.astype(BF16).astype(F32)

    back = []
    for d in range(1, E):
        back_out[d] = total[d * cap : (d + 1) * cap, :].astype(BF16)
        c = remote(
            back_out.at[d], back_in.at[me], back_s.at[d - 1], back_r.at[d - 1],
            lax.rem(me - d + E, E), mt,
        )
        c.start()
        back.append(c)
    back_in[me] = total[0:cap, :].astype(BF16)
    for c in stat:
        c.wait_send()
    for c in share:
        c.wait_send()
    for c in sent:
        c.wait_send()
    for j in range(LE):
        to_core[j].wait_send()
        to_hid[j].wait_send()
        for c in to_y[j]:
            c.wait_send()
    for c in back:
        c.wait()
    finder = jnp.where(key_col == lane.astype(F32), 1.0, 0.0)
    mixed = jnp.zeros((n, width), F32)
    for g in range(G):
        part = back_in[g * group_devices].astype(F32)
        for p in range(1, group_devices):
            part += back_in[g * group_devices + p].astype(F32)
        for s in range(cap):
            at = g * cap + s
            mixed += finder[:, at : at + 1] * part[s : s + 1, :]
    out_ref[...] = mixed.astype(BF16)


def per_device(E, T, tokens, norm_gain, norm_bias, group_pick, member_pick, picked_probs,
               gate_weight, up_weight, down_weight):
    n, width = tokens.shape
    LE, _, FF = gate_weight.shape
    half = FF // CORES
    NY = T // CORES
    G = LE * E // EPG
    cap = max(n // 4, (n + G - 1) // G)
    S = G * cap
    R = E * cap
    k = picked_probs.shape[1]
    dma = pltpu.SemaphoreType.DMA
    V = pltpu.VMEM
    scratch = [
        V((n, width), BF16), V((1, width), F32), V((1, width), F32),
        V((n, 1), jnp.int32), V((n, k), jnp.int32), V((n, k), F32),
        V((LE, width, FF), BF16), V((LE, width, FF), BF16), V((LE, FF, width), BF16),
        V((T, S, LANES), F32),
        V((G, cap, LANES), F32), V((E, cap, LANES), F32), V((R, LANES), F32),
        V((G, cap, width), BF16), V((E, cap, width), BF16), V((R, width), F32),
        V((LE, 2, R, half), BF16), V((LE, 2, R, half), BF16),
        V((LE, 2, R, half), BF16), V((LE, NY - 1, 2, R, half), BF16),
        V((LE, 2, R, half), F32),
        V((LE, R, half), BF16), V((LE, R, half), BF16),
        V((E, cap, width), BF16), V((E, cap, width), BF16),
        dma((6,)), dma((3, LE)),
        dma((T - 1,)), dma((T - 1,)), dma((E - 1,)), dma((E - 1,)), dma((E - 1,)), dma((E - 1,)),
        dma((LE,)), dma((LE,)), dma((LE, NY - 1)), dma((LE, NY - 1)), dma((LE,)), dma((LE,)),
        dma((E - 1,)), dma((E - 1,)),
    ]
    anywhere = pl.BlockSpec(memory_space=pl.ANY)
    return pl.pallas_call(
        functools.partial(kernel, E, T, G, cap),
        out_shape=jax.ShapeDtypeStruct((n, width), BF16),
        in_specs=[anywhere] * 9,
        out_specs=pl.BlockSpec(memory_space=pltpu.VMEM),
        scratch_shapes=scratch,
        compiler_params=pltpu.CompilerParams(collective_id=0, has_side_effects=True),
        name="moe_step",
    )(tokens, norm_gain.reshape(1, width), norm_bias.reshape(1, width), group_pick, member_pick,
      picked_probs, gate_weight, up_weight, down_weight)


def solution(mesh):
    placed = (
        P("ep", "tp"), P("tp"), P("tp"), P("ep", None), P("ep", None), P("ep", None),
        P("ep", "tp", None), P("ep", "tp", None), P("ep", None, "tp"),
    )
    body = functools.partial(per_device, mesh.shape["ep"], mesh.shape["tp"])
    return jax.shard_map(body, mesh=mesh, in_specs=placed, out_specs=P("ep", "tp"), check_vma=False)
```

time: 89.5 us -> 31.4 us (0.35)
  waiting for transfers between devices: 42.8 us -> 0 us
  Pallas kernels: 0 us -> 25.9 us
  between operations: 13.5 us -> 0.01 us
  starting transfers between devices: 11.4 us -> 0 us
  blocking collectives: 8.44 us -> 0 us
  matrix products: 6.1 us -> 0 us
  other arithmetic: 2.63 us -> 0 us
  local copies, waits for them, and re-layouts: 4.16 us -> 5.3 us
    psum x1 -> x0, waiting for transfers between devices: 29.3 us -> none  [per_device(): gate_full, up_full = lax.psum((gate_part, up_part), 'tp')]
    pallas_call x0 -> x1, Pallas kernels: none -> 25.9 us  [per_device(): pl.pallas_call(functools.partial(kernel, E, T, G, cap), out_shape=jax.Sha...]
    all_to_all x2 -> x0, waiting for transfers between devices: 13.5 us -> none  [the longest x1 6.78 us: per_device(): lax.all_to_all(outgoing, 'ep', split_axis=0, concat_axis=0, tiled=True)]
    all_to_all x2 -> x0, starting transfers between devices: 11.3 us -> none  [the longest x1 5.81 us: per_device(): lax.all_to_all(outgoing, 'ep', split_axis=0, concat_axis=0, tiled=True)]
    psum x1 -> x0, blocking collectives: 8.44 us -> none  [normalize(): lax.psum((jnp.sum(values, axis=1, keepdims=True), jnp.sum(values * values...]
    dot_general x4 -> x0, matrix products: 6.1 us -> none  [the longest x1 2.18 us: project_down(): jnp.einsum('jrf,jfd->jrd', hidden, down_weight, preferred_element_type=jn...]
    unnamed x7 -> x4, local copies, waits for them, and re-layouts: 1.27 us -> 5.3 us
    gather x7 -> x0, local copies, waits for them, and re-layouts: 1.64 us -> none  [the longest x5 1 us: per_device(): positions = chosen * capacity + jnp.take_along_axis(slots, chosen, axis=1)]
  transfers between devices with their start and end apart: 3 -> 0, of which waited for: 3 -> 0; matrix products, arithmetic and copies ran while one was open for 1% -> 0% of each run, Pallas kernels for 0% -> 0%
where the time goes in v1:
time: 31.4 us; the launch traced here: 31.2 us
  Pallas kernels  25.9 us (82%)
  local copies, waits for them, and re-layouts  5.3 us (17%)
    pallas_call x1, Pallas kernels, per_device(): pl.pallas_call(functools.partial(kernel, E, T, G, cap), out_shape=jax.Sha...  25.9 us
    unnamed x4, local copies, waits for them, and re-layouts  5.3 us

profile of v1, /device:TPU:0, one launch (start us, length us, event | category | flops | bytes accessed | tf_op | source)
XLA Modules:
  0.0 31.2 jit_solution(959890735339777041)
XLA Ops:
  0.0 1.3 %copy.10.group_h = s32[8,1]{1,0:T(8,128)} copy(s32[8,1]{0,1:T(1,128)} %param.12) | data formatting | bytes 64 | tf_op args[3]
  1.3 1.3 %copy.11.member_h = s32[8,4]{1,0:T(8,128)} copy(s32[8,4]{0,1:T(4,128)} %param.13) | data formatting | bytes 256 | tf_op args[4]
  2.7 1.3 %copy.12.probs_h = f32[8,4]{1,0:T(8,128)} copy(f32[8,4]{0,1:T(4,128)} %param.14) | data formatting | bytes 256 | tf_op args[5]
  4.0 25.9 %moe_step.1 = bf16[8,512]{1,0:T(8,128)(2,1)} custom-call(bf16[8,512]{1,0:T(8,128)(2,1)} %tokens_h.1, f32[1,512]{1,0:T(1,128)} %bitcast.2, f32[1,512]{1,0:T(1,128)} %bitcast.3, s32[8,1]{1,0:T(8,128)} %copy.10.group_h, s32[8,4]{1,0:T(8,128)} %copy.11.member_h, f32[8,4]{1,0:T(8,128)} %copy.12.probs_h, bf16[2,512,1024]{2,1,0:T(8,128)(2,1)} %gate_h.1, ...), custom_call_target="tpu_custom_call" | custom-call | tf_op jit(solution)/shard_map/moe_step/pallas_call | solution.py:295
  29.9 1.3 %copy.14 = bf16[8,512]{1,0:T(8,128)(2,1)} copy(bf16[8,512]{1,0:T(8,128)(2,1)} %moe_step.1) | data formatting | bytes 16384

commit v2 on v1

--- a/solution.py
+++ b/solution.py
@@ -83,17 +83,21 @@
     for c in small:
         c.wait()
 
-    lane = iota((n, LANES), 1)
-    sub = iota((n, LANES), 0)
-    group = group_v[...].astype(F32)
-    group_wide = jnp.broadcast_to(group, (n, LANES))
-    group_row = jnp.sum(jnp.where(lane == sub, group_wide, 0.0), axis=0, keepdims=True)
-    same = jnp.where(group_wide == group_row, 1.0, 0.0)
+    lane = iota((n, n), 1)
+    sub = iota((n, n), 0)
+
+    def column(row):
+        wide = jnp.broadcast_to(row, (n, n))
+        return jnp.sum(jnp.where(lane == sub, wide, 0.0), axis=1, keepdims=True)
+
+    group_row = group_v[...].astype(F32)
+    group_col = column(group_row)
+    same = jnp.where(group_col == group_row, 1.0, 0.0)
     slot_row = jnp.sum(jnp.where(sub < lane, same, 0.0), axis=0, keepdims=True)
     slot_col = jnp.sum(jnp.where(lane < sub, same, 0.0), axis=1, keepdims=True)
-    key_row = jnp.where(iota((1, LANES), 1) < n, group_row * cap + slot_row, -1.0)
-    key_col = group * cap + slot_col
-    place = jnp.where(key_row == iota((S, LANES), 0).astype(F32), 1.0, 0.0)
+    key_row = group_row * cap + slot_row
+    key_col = group_col * cap + slot_col
+    place = jnp.where(key_row == iota((S, n), 0).astype(F32), 1.0, 0.0)
 
     def pack(v):
         total = place[:, 0:1] * v[0:1, :]
@@ -102,11 +106,13 @@
         return total
 
     probs = probs_v[...]
-    member = member_v[...]
-    shares = probs / jnp.sum(probs, axis=1, keepdims=True)
+    member = member_v[...].astype(F32)
+    shares = probs / jnp.sum(probs, axis=0, keepdims=True)
+    share_lane = iota((n, LANES), 1).astype(F32)
     share_tile = jnp.zeros((n, LANES), F32)
-    for k in range(probs.shape[1]):
-        share_tile += jnp.where(lane == member[:, k : k + 1], shares[:, k : k + 1], 0.0)
+    for k in range(probs.shape[0]):
+        hit = share_lane == column(member[k : k + 1, :])
+        share_tile += jnp.where(hit, column(shares[k : k + 1, :]), 0.0)
     share_tile = pack(share_tile)
     for g in range(G):
         share_out[g] = share_tile[g * cap : (g + 1) * cap, :]
@@ -249,7 +255,7 @@
             c.wait_send()
     for c in back:
         c.wait()
-    finder = jnp.where(key_col == lane.astype(F32), 1.0, 0.0)
+    finder = jnp.where(key_col == iota((n, LANES), 1).astype(F32), 1.0, 0.0)
     mixed = jnp.zeros((n, width), F32)
     for g in range(G):
         part = back_in[g * group_devices].astype(F32)
@@ -258,7 +264,7 @@
         for s in range(cap):
             at = g * cap + s
             mixed += finder[:, at : at + 1] * part[s : s + 1, :]
-    out_ref[...] = mixed.astype(BF16)
+    out_ref[...] = mixed
 
 
 def per_device(E, T, tokens, norm_gain, norm_bias, group_pick, member_pick, picked_probs,
@@ -276,7 +282,7 @@
     V = pltpu.VMEM
     scratch = [
         V((n, width), BF16), V((1, width), F32), V((1, width), F32),
-        V((n, 1), jnp.int32), V((n, k), jnp.int32), V((n, k), F32),
+        V((1, n), jnp.int32), V((k, n), jnp.int32), V((k, n), F32),
         V((LE, width, FF), BF16), V((LE, width, FF), BF16), V((LE, FF, width), BF16),
         V((T, S, LANES), F32),
         V((G, cap, LANES), F32), V((E, cap, LANES), F32), V((R, LANES), F32),
@@ -291,17 +297,18 @@
         dma((LE,)), dma((LE,)), dma((LE, NY - 1)), dma((LE, NY - 1)), dma((LE,)), dma((LE,)),
         dma((E - 1,)), dma((E - 1,)),
     ]
-    anywhere = pl.BlockSpec(memory_space=pl.ANY)
-    return pl.pallas_call(
+    anywhere = pl.BlockSpec(memory_space=pltpu.HBM)
+    combined = pl.pallas_call(
         functools.partial(kernel, E, T, G, cap),
-        out_shape=jax.ShapeDtypeStruct((n, width), BF16),
+        out_shape=jax.ShapeDtypeStruct((n, width), F32),
         in_specs=[anywhere] * 9,
         out_specs=pl.BlockSpec(memory_space=pltpu.VMEM),
         scratch_shapes=scratch,
-        compiler_params=pltpu.CompilerParams(collective_id=0, has_side_effects=True),
+        compiler_params=pltpu.CompilerParams(collective_id=0, has_side_effects=True, vmem_limit_bytes=32 * 1024 * 1024),
         name="moe_step",
-    )(tokens, norm_gain.reshape(1, width), norm_bias.reshape(1, width), group_pick, member_pick,
-      picked_probs, gate_weight, up_weight, down_weight)
+    )(tokens, norm_gain.reshape(1, width), norm_bias.reshape(1, width), group_pick.T, member_pick.T,
+      picked_probs.T, gate_weight, up_weight, down_weight)
+    return combined.astype(BF16)
 
 
 def solution(mesh):

time: 31.4 us -> 35 us (1.11)
  local copies, waits for them, and re-layouts: 5.3 us -> 8.85 us
  Pallas kernels: 25.9 us -> 25.2 us
  other arithmetic: 0 us -> 0.6 us
    unnamed x4 -> x18, local copies, waits for them, and re-layouts: 5.3 us -> 8.85 us
    pallas_call x1, Pallas kernels: 25.9 us -> 25.2 us  [per_device(): pl.pallas_call(functools.partial(kernel, E, T, G, cap), out_shape=jax.Sha...]
    convert_element_type x0 -> x1, other arithmetic: none -> 0.6 us  [per_device(): return combined.astype(BF16)]
where the time goes in v2:
time: 35 us; the launch traced here: 34.7 us
  Pallas kernels  25.2 us (72%)
  local copies, waits for them, and re-layouts  8.85 us (25%)
  other arithmetic  0.6 us (2%)
    pallas_call x1, Pallas kernels, per_device(): pl.pallas_call(functools.partial(kernel, E, T, G, cap), out_shape=jax.Sha...  25.2 us
    unnamed x18, local copies, waits for them, and re-layouts  8.85 us

profile of v2, /device:TPU:0, one launch (start us, length us, event | category | flops | bytes accessed | tf_op | source)
XLA Modules:
  0.0 34.7 jit_solution(179396246825422751)
XLA Ops:
  0.0 0.0 copy-start
  0.0 1.6 %copy-done = bf16[2,512,1024]{2,1,0:T(8,128)(2,1)S(1)} copy-done((bf16[2,512,1024]{2,1,0:T(8,128)(2,1)S(1)}, bf16[2,512,1024]{2,1,0:T(8,128)(2,1)}, u32[]{:S(2)}) %copy-start) | copy-done | bytes 2097176
  1.6 0.0 copy-start.1
  1.6 1.6 %copy-done.1 = bf16[2,512,1024]{2,1,0:T(8,128)(2,1)S(1)} copy-done((bf16[2,512,1024]{2,1,0:T(8,128)(2,1)S(1)}, bf16[2,512,1024]{2,1,0:T(8,128)(2,1)}, u32[]{:S(2)}) %copy-start.1) | copy-done | bytes 2097176
  3.2 0.0 copy-start.2
  3.2 1.6 %copy-done.2 = bf16[2,1024,512]{2,1,0:T(8,128)(2,1)S(1)} copy-done((bf16[2,1024,512]{2,1,0:T(8,128)(2,1)S(1)}, bf16[2,1024,512]{2,1,0:T(8,128)(2,1)}, u32[]{:S(2)}) %copy-start.2) | copy-done | bytes 2097176
  4.8 0.0 copy-start.3
  4.8 0.7 %copy-done.3 = bf16[8,512]{1,0:T(8,128)(2,1)S(1)} copy-done((bf16[8,512]{1,0:T(8,128)(2,1)S(1)}, bf16[8,512]{1,0:T(8,128)(2,1)}, u32[]{:S(2)}) %copy-start.3) | copy-done | bytes 8216
  5.5 0.0 copy-start.4
  5.5 0.7 %copy-done.4 = f32[512]{0:T(512)S(1)} copy-done((f32[512]{0:T(512)S(1)}, f32[512]{0:T(512)}, u32[]{:S(2)}) %copy-start.4) | copy-done | bytes 2072
  6.2 0.0 copy-start.5
  6.2 0.7 %copy-done.5 = f32[512]{0:T(512)S(1)} copy-done((f32[512]{0:T(512)S(1)}, f32[512]{0:T(512)}, u32[]{:S(2)}) %copy-start.5) | copy-done | bytes 2072
  6.8 0.0 copy-start.6
  6.8 0.7 %copy-done.6 = s32[8,4]{0,1:T(4,128)S(1)} copy-done((s32[8,4]{0,1:T(4,128)S(1)}, s32[8,4]{0,1:T(4,128)}, u32[]{:S(2)}) %copy-start.6) | copy-done | bytes 152
  7.5 0.0 copy-start.7
  7.5 0.7 %copy-done.7 = f32[8,4]{0,1:T(4,128)S(1)} copy-done((f32[8,4]{0,1:T(4,128)S(1)}, f32[8,4]{0,1:T(4,128)}, u32[]{:S(2)}) %copy-start.7) | copy-done | bytes 152
  8.2 0.0 copy-start.8
  8.2 0.7 %copy-done.8 = s32[8,1]{0,1:T(1,128)S(1)} copy-done((s32[8,1]{0,1:T(1,128)S(1)}, s32[8,1]{0,1:T(1,128)}, u32[]{:S(2)}) %copy-start.8) | copy-done | bytes 56
  8.9 25.2 %moe_step.1 = f32[8,512]{1,0:T(8,128)S(1)} custom-call(bf16[8,512]{1,0:T(8,128)(2,1)S(1)} %copy-done.3, f32[1,512]{1,0:T(1,128)S(1)} %bitcast.5, f32[1,512]{1,0:T(1,128)S(1)} %bitcast.6, s32[1,8]{1,0:T(1,128)S(1)} %bitcast.9, s32[4,8]{1,0:T(4,128)S(1)} %bitcast.7, f32[4,8]{1,0:T(4,128)S(1)} %bitcast.8, bf16[2,512,1024]{2,1,0:T(8,128)(2,1)S(1)} %copy-done, ...), custom_call_target="tpu_custom_call" | custom-call | tf_op jit(solution)/shard_map/moe_step/pallas_call | solution.py:301
  34.1 0.6 %convert_element_type.3 = bf16[8,512]{1,0:T(8,128)(2,1)} convert(f32[8,512]{1,0:T(8,128)S(1)} %moe_step.1) | non-fusion elementwise | flops 4096 | bytes 24576 | tf_op jit(solution)/shard_map/convert_element_type | solution.py:311
Async XLA Ops:
  0.0 1.6 %copy-start = (bf16[2,512,1024]{2,1,0:T(8,128)(2,1)S(1)}, bf16[2,512,1024]{2,1,0:T(8,128)(2,1)}, u32[]{:S(2)}) copy-start(bf16[2,512,1024]{2,1,0:T(8,128)(2,1)} %gate_h.1) | copy-start | bytes 6291460
  1.6 1.6 %copy-start.1 = (bf16[2,512,1024]{2,1,0:T(8,128)(2,1)S(1)}, bf16[2,512,1024]{2,1,0:T(8,128)(2,1)}, u32[]{:S(2)}) copy-start(bf16[2,512,1024]{2,1,0:T(8,128)(2,1)} %up_h.1) | copy-start | bytes 6291460
  3.2 1.6 %copy-start.2 = (bf16[2,1024,512]{2,1,0:T(8,128)(2,1)S(1)}, bf16[2,1024,512]{2,1,0:T(8,128)(2,1)}, u32[]{:S(2)}) copy-start(bf16[2,1024,512]{2,1,0:T(8,128)(2,1)} %down_h.1) | copy-start | bytes 6291460
  4.8 0.7 %copy-start.3 = (bf16[8,512]{1,0:T(8,128)(2,1)S(1)}, bf16[8,512]{1,0:T(8,128)(2,1)}, u32[]{:S(2)}) copy-start(bf16[8,512]{1,0:T(8,128)(2,1)} %tokens_h.1) | copy-start | bytes 24580
  5.5 0.7 %copy-start.4 = (f32[512]{0:T(512)S(1)}, f32[512]{0:T(512)}, u32[]{:S(2)}) copy-start(f32[512]{0:T(512)} %param.10) | copy-start | bytes 6148
  6.2 0.7 %copy-start.5 = (f32[512]{0:T(512)S(1)}, f32[512]{0:T(512)}, u32[]{:S(2)}) copy-start(f32[512]{0:T(512)} %param.11) | copy-start | bytes 6148
  6.8 0.7 %copy-start.6 = (s32[8,4]{0,1:T(4,128)S(1)}, s32[8,4]{0,1:T(4,128)}, u32[]{:S(2)}) copy-start(s32[8,4]{0,1:T(4,128)} %param.13) | copy-start | bytes 388
  7.5 0.7 %copy-start.7 = (f32[8,4]{0,1:T(4,128)S(1)}, f32[8,4]{0,1:T(4,128)}, u32[]{:S(2)}) copy-start(f32[8,4]{0,1:T(4,128)} %param.14) | copy-start | bytes 388
  8.2 0.7 %copy-start.8 = (s32[8,1]{0,1:T(1,128)S(1)}, s32[8,1]{0,1:T(1,128)}, u32[]{:S(2)}) copy-start(s32[8,1]{0,1:T(1,128)} %param.12) | copy-start | bytes 100

commit v3 on v2

--- a/solution.py
+++ b/solution.py
@@ -297,14 +297,14 @@
         dma((LE,)), dma((LE,)), dma((LE, NY - 1)), dma((LE, NY - 1)), dma((LE,)), dma((LE,)),
         dma((E - 1,)), dma((E - 1,)),
     ]
-    anywhere = pl.BlockSpec(memory_space=pltpu.HBM)
+    anywhere = pl.BlockSpec(memory_space=pl.ANY)
     combined = pl.pallas_call(
         functools.partial(kernel, E, T, G, cap),
         out_shape=jax.ShapeDtypeStruct((n, width), F32),
         in_specs=[anywhere] * 9,
         out_specs=pl.BlockSpec(memory_space=pltpu.VMEM),
         scratch_shapes=scratch,
-        compiler_params=pltpu.CompilerParams(collective_id=0, has_side_effects=True, vmem_limit_bytes=32 * 1024 * 1024),
+        compiler_params=pltpu.CompilerParams(collective_id=0, has_side_effects=True),
         name="moe_step",
     )(tokens, norm_gain.reshape(1, width), norm_bias.reshape(1, width), group_pick.T, member_pick.T,
       picked_probs.T, gate_weight, up_weight, down_weight)

time: 35 us -> 27.4 us (0.78)
  local copies, waits for them, and re-layouts: 8.85 us -> 0 us
  other arithmetic: 0.6 us -> 1.32 us
  Pallas kernels: 25.2 us -> 25.8 us
    unnamed x18 -> x0, local copies, waits for them, and re-layouts: 8.85 us -> none
    convert_element_type x1, other arithmetic: 0.6 us -> 1.32 us  [per_device(): return combined.astype(BF16)]
    pallas_call x1, Pallas kernels: 25.2 us -> 25.8 us  [per_device(): pl.pallas_call(functools.partial(kernel, E, T, G, cap), out_shape=jax.Sha...]
where the time goes in v3:
time: 27.4 us; the launch traced here: 27.1 us
  Pallas kernels  25.8 us (94%)
  other arithmetic  1.32 us (5%)
    pallas_call x1, Pallas kernels, per_device(): pl.pallas_call(functools.partial(kernel, E, T, G, cap), out_shape=jax.Sha...  25.8 us
    convert_element_type x1, other arithmetic, per_device(): return combined.astype(BF16)  1.32 us

profile of v3, /device:TPU:0, one launch (start us, length us, event | category | flops | bytes accessed | tf_op | source)
XLA Modules:
  0.0 27.1 jit_solution(8432084776294599522)
XLA Ops:
  0.0 25.8 %moe_step.1 = f32[8,512]{1,0:T(8,128)} custom-call(bf16[8,512]{1,0:T(8,128)(2,1)} %tokens_h.1, f32[1,512]{1,0:T(1,128)} %bitcast.5, f32[1,512]{1,0:T(1,128)} %bitcast.6, s32[1,8]{1,0:T(1,128)} %bitcast.9, s32[4,8]{1,0:T(4,128)} %bitcast.7, f32[4,8]{1,0:T(4,128)} %bitcast.8, bf16[2,512,1024]{2,1,0:T(8,128)(2,1)} %gate_h.1, bf16[2,512,1024]{2,1,0:T(8,128)(2,1)} %up_h.1, ...), custom_call_target="tpu_custom_call" | custom-call | tf_op jit(solution)/shard_map/moe_step/pallas_call | solution.py:301
  25.8 1.3 %convert_element_type.3 = bf16[8,512]{1,0:T(8,128)(2,1)} convert(f32[8,512]{1,0:T(8,128)} %moe_step.1) | non-fusion elementwise | flops 4096 | bytes 24576 | tf_op jit(solution)/shard_map/convert_element_type | solution.py:311
